TPU v7x, 32 devices: a whole 2x2x4 slice. The times are simulated.
32 devices in a mesh: sp: 16 (over z, y, x), tp: 2 (over core).
Axes of the slice: x: 2, y: 2, z: 4, core: 2. Of those that a mesh axis runs over, the one named last changes fastest.
Arguments:
- prompt: bfloat16 [16, 1024, 2048], P('sp', None, 'tp'), may hold values from -6 to 6
- new_input: bfloat16 [16, 2048], P('sp', 'tp'), may hold values from -140 to 140
- w_query: bfloat16 [2048, 2048], P('sp', 'tp'), may hold values from -0.21875 to 0.21875
- w_key: bfloat16 [2048, 2048], P('sp', 'tp'), may hold values from -0.125 to 0.125
- w_value: bfloat16 [2048, 2048], P('sp', 'tp'), may hold values from -0.125 to 0.125
- lam: float32 [16], P('tp'), may hold values from 0.3 to 0.8
- out_gain: float32 [128], replicated, may hold values from 0.1 to 1.9
Outputs:
- key_cache: bfloat16 [16, 1024, 2048], P('sp', None, 'tp')
- value_cache: bfloat16 [16, 1024, 2048], P('sp', None, 'tp')
- first_read: bfloat16 [16, 16, 128], P('sp', 'tp')
All inputs are finite; a program needn't handle non-finite values.
Results may differ from a plain program's by a relative error of at most 0.02.
The roundings to bfloat16 on the way count: a program that leaves them out, or rounds other values in their place, can miss the bound.
Values may be sent and summed in bfloat16 or wider, within the bound.
A program may use at most 64 MiB of HBM per device.

v0:
```python
import jax
import jax.numpy as jnp
from jax import lax
from jax.sharding import PartitionSpec as P

MAP_DIM = 64
VAL_DIM = 128
LEN = 1024


rope_base = 500000.0
norm_eps = 1e-05


def rotate(vectors, angle):
    half = vectors.shape[-1] // 2
    cosine_table = jnp.cos(angle)
    sine = jnp.sin(angle)
    first = vectors[..., :half]
    second = vectors[..., half:]
    return jnp.concatenate(
        [first * cosine_table - second * sine, second * cosine_table + first * sine], axis=-1
    )


def inverse_freq():
    return rope_base ** (-(jnp.arange(MAP_DIM // 2, dtype=jnp.float32) * 2.0 / MAP_DIM))


def finish(mixed, lam, out_gain):
    diff = mixed[:, :, 0] - lam[None, :, None] * mixed[:, :, 1]
    normed = diff * lax.rsqrt(jnp.mean(diff * diff, axis=-1, keepdims=True) + norm_eps)
    return (normed * out_gain).astype(jnp.bfloat16)


def read_whole(query, keys, values, lam, out_gain):
    seqs, length, _ = keys.shape
    heads = lam.shape[0]
    key_maps = keys.reshape(seqs, length, heads, 2, MAP_DIM)
    value_heads = values.reshape(seqs, length, heads, VAL_DIM)
    attention_scores = jnp.einsum(
        "shmd,slhmd->shml", query, key_maps, preferred_element_type=jnp.float32
    ) * MAP_DIM ** (-0.5)
    weights = jax.nn.softmax(attention_scores, axis=-1)
    mixed = jnp.einsum(
        "shml,slhe->shme", weights, value_heads.astype(jnp.float32), precision=lax.Precision.HIGHEST
    )
    return finish(mixed, lam, out_gain)


def body(prompt, new_input, w_query, w_key, w_value, lam, out_gain):
    heads = lam.shape[0]
    seqs, count, _ = prompt.shape
    local_seqs = new_input.shape[0]
    inverse = inverse_freq()
    full_query, full_key, full_value = (
        lax.all_gather(w_query, "sp", axis=0, tiled=True),
        lax.all_gather(w_key, "sp", axis=0, tiled=True),
        lax.all_gather(w_value, "sp", axis=0, tiled=True),
    )
    pieces = (
        lax.all_gather(prompt, "tp", axis=2, tiled=True),
        lax.all_gather(new_input[:, None, :], "tp", axis=2, tiled=True),
    )
    width_piece = pieces[0].shape[2]
    row_piece = pieces[0].reshape(seqs * count, width_piece)
    fresh_piece = pieces[1][:, 0, :]
    key_sum = jnp.dot(row_piece, full_key, preferred_element_type=jnp.float32)
    weighted_value_sum = jnp.dot(row_piece, full_value, preferred_element_type=jnp.float32)
    query_sum = jnp.dot(fresh_piece, full_query, preferred_element_type=jnp.float32)
    positions = jnp.arange(count, dtype=jnp.float32)
    key_maps = rotate(
        key_sum.reshape(seqs, count, heads, 2, MAP_DIM), positions[:, None, None, None] * inverse
    )
    keys = key_maps.astype(jnp.bfloat16).reshape(seqs, count, heads * 2 * MAP_DIM)
    values = weighted_value_sum.astype(jnp.bfloat16).reshape(seqs, count, heads * VAL_DIM)
    query = rotate(
        query_sum.reshape(local_seqs, heads, 2, MAP_DIM), jnp.float32(LEN) * inverse
    ).astype(jnp.bfloat16)
    first_read = read_whole(query, keys, values, lam, out_gain)
    return (keys, values, first_read)


def solution(mesh):
    in_specs = (
        P("sp", None, "tp"),
        P("sp", "tp"),
        P("sp", "tp"),
        P("sp", "tp"),
        P("sp", "tp"),
        P("tp"),
        P(),
    )
    out_specs = (P("sp", None, "tp"), P("sp", None, "tp"), P("sp", "tp", None))
    return jax.shard_map(body, mesh=mesh, in_specs=in_specs, out_specs=out_specs, check_vma=False)
```

profile of v0, /device:TPU:0, one launch (start us, length us, event | category | flops | bytes accessed | tf_op | source)
XLA Modules:
  0.0 297.6 jit_solution(11442602501516390730)
XLA Ops:
  7.2 0.0 all-gather.8.cloned.1.call-start
  7.2 0.7 all-gather.8.cloned.1.call-update
  7.9 0.0 all-gather.12.cloned.1.call-start
  7.9 1.8 copy.16
  9.7 0.0 all-gather.12.cloned.1.call-update
  9.8 0.0 all-gather.6.cloned.1.call-start
  9.8 0.7 all-gather.6.cloned.1.call-update
  10.5 0.0 all-gather.10.cloned.1.call-start
  10.5 0.5 all-gather.10.cloned.1.call-update
  11.1 2.1 all-gather
  13.2 0.1 multiply_sine_fusion
  13.2 0.5 fusion.15
  13.8 75.3 %all-gather.8.cloned.1.call-done = bf16[2048,1024]{1,0:T(8,128)(2,1)} async-done(((bf16[128,1024]{1,0:T(8,128)(2,1)}), bf16[2048,1024]{1,0:T(8,128)(2,1)}) %all-gather.8.cloned.1.call-update) | async-done | bytes 4194320 | tf_op jit(solution)/shard_map/all_gather | solution.py:58
  89.1 6.5 %copy.15 = bf16[1024,2048]{1,0:T(8,128)(2,1)} copy(bf16[1024,2048]{0,1:T(8,128)(2,1)} %bitcast.59) | data formatting | bytes 8388608 | tf_op jit(solution)/shard_map/dot_general | solution.py:68
  95.6 84.1 %all-gather.12.cloned.1.call-done = bf16[2048,1024]{0,1:T(8,128)(2,1)} async-done(((bf16[128,1024]{0,1:T(8,128)(2,1)}), bf16[2048,1024]{0,1:T(8,128)(2,1)}) %all-gather.12.cloned.1.call-update) | async-done | bytes 4194320 | tf_op jit(solution)/shard_map/all_gather | solution.py:57
  179.7 3.9 %fusion.20 = f32[1,8,2,64]{3,0,2,1:T(1,128)S(1)} fusion(bf16[8,2,64,2048]{3,2,1,0:T(8,128)(2,1)} %bitcast.60, bf16[1,2048]{1,0:T(2,128)(2,1)S(1)} %all-gather), kind=kOutput, calls=%fused_computation.23 | convolution fusion | flops 4194304 | bytes 4202496 | tf_op jit(solution)/shard_map/dot_general | solution.py:70
  183.6 0.1 fusion.23
  183.7 0.1 maximum_bitcast_fusion
  183.8 9.3 %all-gather.6.cloned.1.call-done = bf16[1,1024,2048]{2,1,0:T(8,128)(2,1)} async-done(((bf16[1,1024,1024]{2,1,0:T(8,128)(2,1)}), bf16[1,1024,2048]{2,1,0:T(8,128)(2,1)}) %all-gather.6.cloned.1.call-update) | async-done | bytes 4194320 | tf_op jit(solution)/shard_map/all_gather | solution.py:62
  193.1 7.6 %fusion.4 = f32[1,1024,8,2,64]{1,4,3,2,0:T(8,128)S(1)} fusion(bf16[8,2,64,2048]{3,2,1,0:T(8,128)(2,1)} %bitcast.61, bf16[1,1024,2048]{2,1,0:T(8,128)(2,1)} %all-gather.6.cloned.1.call-done), kind=kOutput, calls=%fused_computation.4 | convolution fusion | flops 4294967296 | bytes 12582912 | tf_op jit(solution)/shard_map/dot_general | solution.py:68
  200.7 0.7 subtract_convert_fusion
  201.5 0.4 fusion.7
  201.9 0.1 fusion.25
  202.0 0.2 fusion.17
  202.2 0.2 pad_maximum_fusion
  202.4 0.0 copy-start.1
  202.4 70.2 %all-gather.10.cloned.1.call-done = bf16[2048,1024]{1,0:T(8,128)(2,1)} async-done(((bf16[128,1024]{1,0:T(8,128)(2,1)}), bf16[2048,1024]{1,0:T(8,128)(2,1)}) %all-gather.10.cloned.1.call-update) | async-done | bytes 4194320 | tf_op jit(solution)/shard_map/all_gather | solution.py:59
  272.6 8.0 %fusion.11 = bf16[1024,1024]{0,1:T(8,128)(2,1)S(1)} fusion(bf16[2048,1024]{1,0:T(8,128)(2,1)} %all-gather.10.cloned.1.call-done, bf16[1,1024,2048]{2,1,0:T(8,128)(2,1)} %all-gather.6.cloned.1.call-done), kind=kOutput, calls=%fused_computation.12 | convolution fusion | flops 4296015872 | bytes 10485760 | tf_op jit(solution)/shard_map/dot_general | solution.py:69
  280.6 0.0 copy-start
  280.6 1.3 copy-done
  281.9 1.8 convolution_bitcast_fusion
  283.7 0.0 copy-done.1
  283.7 0.2 multiply_reduce_fusion
  283.9 0.0 copy-start.2
  283.9 2.6 copy.19
  286.5 3.9 %copy.20 = bf16[1,1024,1024]{2,1,0:T(8,128)(2,1)} copy(bf16[1,1024,1024]{1,2,0:T(8,128)(2,1)} %bitcast.65) | data formatting | bytes 4194304
  290.4 0.0 copy-done.2
  290.4 0.7 multiply_convert_fusion
  (3 shorter events, 0.0 us)
Async XLA Ops:
  7.2 81.9 %all-gather.8.cloned.1.call-start = ((), (), s32[]{:S(2)}) async-start(), calls=%async_computation.1 | async-start | bytes 4456448 | tf_op jit(solution)/shard_map/all_gather | solution.py:58
  7.9 171.8 %all-gather.12.cloned.1.call-start = ((), (), s32[]{:S(2)}) async-start(), calls=%async_computation.3 | async-start | bytes 4456448 | tf_op jit(solution)/shard_map/all_gather | solution.py:57
  9.8 183.4 %all-gather.6.cloned.1.call-start = ((), (), s32[]{:S(2)}) async-start(), calls=%async_computation | async-start | bytes 6291456 | tf_op jit(solution)/shard_map/all_gather | solution.py:62
  10.5 262.1 %all-gather.10.cloned.1.call-start = ((), (), s32[]{:S(2)}) async-start(), calls=%async_computation.2 | async-start | bytes 4456448 | tf_op jit(solution)/shard_map/all_gather | solution.py:59
  202.4 81.3 %copy-start.1 = (f32[8]{0:T(128)S(1)}, f32[8]{0:T(128)}, u32[]{:S(2)}) copy-start(f32[8]{0:T(128)} %param.12) | copy-start | bytes 100
  280.6 1.3 copy-start
  283.9 6.5 %copy-start.2 = (f32[128]{0:T(128)S(1)}, f32[128]{0:T(128)}, u32[]{:S(2)}) copy-start(f32[128]{0:T(128)} %param.13) | copy-start | bytes 1540
Sparse Core Ops, SparseCore 0:
  10.7 78.3 all-gather.7
  92.4 87.3 all-gather.11
  181.3 11.8 all-gather.5
  195.8 76.7 all-gather.9
where the time goes:
time: 298 us
  waiting for transfers between devices  241 us (81%)
  matrix products  21.7 us (7%)
  local copies, waits for them, and re-layouts  16.1 us (5%)
  between operations  13.9 us (5%)
    all_gather x1, waiting for transfers between devices, body(): lax.all_gather(w_query, 'sp', axis=0, tiled=True)  84.1 us
    all_gather x1, waiting for transfers between devices, body(): lax.all_gather(w_key, 'sp', axis=0, tiled=True)  75.3 us
    all_gather x1, waiting for transfers between devices, body(): lax.all_gather(w_value, 'sp', axis=0, tiled=True)  70.2 us
    unnamed x9, local copies, waits for them, and re-layouts  9.62 us
    all_gather x1, waiting for transfers between devices, body(): lax.all_gather(prompt, 'tp', axis=2, tiled=True)  9.34 us
    dot_general x1, matrix products, body(): jnp.dot(row_piece, full_value, preferred_element_type=jnp.float32)  8.02 us
    dot_general x1, matrix products, body(): key_sum = jnp.dot(row_piece, full_key, preferred_element_type=jnp.float32)  7.59 us
    dot_general x1, local copies, waits for them, and re-layouts, body(): key_sum = jnp.dot(row_piece, full_key, preferred_element_type=jnp.float32)  6.5 us
  transfers between devices with their start and end apart: 4, of which 4 were waited for; matrix products, arithmetic and copies ran while one was open for 7% of the time, Pallas kernels for 0%

commit v1 on v0

v1 whole, which is shorter than its diff:
```python
import functools

import jax
import jax.numpy as jnp
from jax import lax
from jax.experimental import pallas as pl
from jax.experimental.pallas import tpu as pltpu
from jax.sharding import PartitionSpec as P

MAP_DIM = 64
VAL_DIM = 128
LANES = 128
rope_base = 500000.0
norm_eps = 1e-05

X, Y, UP, DOWN = 0, 1, 2, 3
F32, BF16 = jnp.float32, jnp.bfloat16


def inverse_freq():
    return rope_base ** (-(jnp.arange(MAP_DIM // 2, dtype=F32) * 2.0 / MAP_DIM))


def tables(positions):
    angle = positions[:, None] * inverse_freq()
    cosine, sine = jnp.cos(angle), jnp.sin(angle)
    reps = LANES // MAP_DIM
    return (
        jnp.concatenate([cosine, cosine] * reps, axis=-1),
        jnp.concatenate([-sine, sine] * reps, axis=-1),
    )


def rotated(tile, cosine, sine):
    half = MAP_DIM // 2
    lane = lax.broadcasted_iota(jnp.int32, tile.shape, 1) % MAP_DIM
    other = jnp.where(lane < half, pltpu.roll(tile, LANES - half, 1), pltpu.roll(tile, half, 1))
    return tile * cosine + other * sine


def kernel(
    n, tp, prompt, fresh, wq, wk, wv, cos_t, sin_t, qcos, qsin, lam, gain,
    k_out, v_out, read_out,
    W, PR, acc, ko, vo, XN, XM, wq_v, QS, QR, ct, st,
    w_recv, w_send, p_recv, p_send, x_recv, x_send, xt_recv, xt_send, q_recv, q_send, loc,
):
    _, rows, wl = prompt.shape
    depth, cols = wk.shape
    half = cols // 2
    heads = cols // VAL_DIM
    L = n // 4
    plane = 4 * depth
    me, mt = lax.axis_index("sp"), lax.axis_index("tp")
    z, y, x = me // 4, (me // 2) % 2, me % 2
    yf, xf = 1 - y, 1 - x

    def at(zo, yo, xo):
        return zo * 4 + yo * 2 + xo

    partner = {X: at(z, y, xf), Y: at(z, yf, x), UP: me + 4, DOWN: me - 4}

    def piece(c, o):
        return W.at[c, pl.ds(pl.multiple_of(o * depth, depth), depth), :]

    def copy(c, d, o):
        return pltpu.make_async_remote_copy(
            src_ref=piece(c, o), dst_ref=piece(c, o),
            send_sem=w_send.at[(c * 4 + d) * n + o], recv_sem=w_recv.at[c * n + o],
            device_id={"sp": partner[d]}, device_id_type=pl.DeviceIdType.MESH,
        )

    def send(c, d, o):
        copy(c, d, o).start()

    def got(c, o):
        copy(c, X, o).wait_recv()

    barrier = pltpu.get_barrier_semaphore()
    for d in range(1, tp):
        pl.semaphore_signal(
            barrier, inc=1, device_id={"tp": (mt + d) % tp}, device_id_type=pl.DeviceIdType.MESH)

    def greet(d, _):
        pl.semaphore_signal(
            barrier, inc=1, device_id={"sp": (me + d) % n}, device_id_type=pl.DeviceIdType.MESH)
        return _

    lax.fori_loop(1, n, greet, 0)

    def columns(t):
        return PR.at[:, pl.ds(pl.multiple_of(t * wl, wl), wl)]

    own = [
        pltpu.make_async_copy(w.at[:, pl.ds(h * half, half)], piece(2 * i + h, me), loc.at[2 * i + h])
        for i, w in enumerate((wk, wv)) for h in range(2)
    ]
    rest = [
        pltpu.make_async_copy(fresh, XN.at[mt, me], loc.at[4]),
        pltpu.make_async_copy(prompt.at[0], columns(mt), loc.at[5]),
        pltpu.make_async_copy(wq, wq_v, loc.at[6]),
        pltpu.make_async_copy(cos_t, ct, loc.at[7]),
        pltpu.make_async_copy(sin_t, st, loc.at[8]),
    ]
    rest[0].start()
    for c in own:
        c.start()
    for c in rest[1:]:
        c.start()
    rest[0].wait()
    for c in own:
        c.wait()
    pl.semaphore_wait(barrier, n - 1 + tp - 1)

    def x_copy(d):
        return pltpu.make_async_remote_copy(
            src_ref=XN.at[mt, me], dst_ref=XN.at[mt, me],
            send_sem=x_send.at[d], recv_sem=x_recv.at[me],
            device_id={"sp": (me + d) % n}, device_id_type=pl.DeviceIdType.MESH,
        )

    def x_wait(d):
        src = (me + d) % n
        return pltpu.make_async_remote_copy(
            src_ref=XN.at[mt, src], dst_ref=XN.at[mt, src],
            send_sem=x_send.at[d], recv_sem=x_recv.at[src],
            device_id={"sp": src}, device_id_type=pl.DeviceIdType.MESH,
        )

    def loop(lo, hi, f):
        lax.fori_loop(lo, hi, lambda i, _: (f(i), _)[1], 0)

    loop(1, n, lambda d: x_copy(d).start())

    up_ok, down_ok = z + 1 < L, z > 0

    def along_z(c, o):
        @pl.when(up_ok)
        def _():
            send(c, UP, o)

        @pl.when(down_ok)
        def _():
            send(c, DOWN, o)

    send(0, Y, me)
    send(1, X, me)
    for c in range(4):
        along_z(c, me)
    send(2, X, me)
    send(3, Y, me)
    send(0, X, me)
    send(1, Y, me)
    send(2, Y, me)
    send(3, X, me)

    def p_copy(d):
        return pltpu.make_async_remote_copy(
            src_ref=prompt.at[0], dst_ref=columns(mt),
            send_sem=p_send.at[d], recv_sem=p_recv.at[mt],
            device_id={"tp": (mt + d) % tp}, device_id_type=pl.DeviceIdType.MESH,
        )

    def p_wait(d):
        src = (mt + d) % tp
        return pltpu.make_async_remote_copy(
            src_ref=columns(src), dst_ref=columns(src),
            send_sem=p_send.at[d], recv_sem=p_recv.at[src],
            device_id={"tp": src}, device_id_type=pl.DeviceIdType.MESH,
        )

    for d in range(1, tp):
        p_copy(d).start()

    o_y, o_x = at(z, yf, x), at(z, y, xf)
    got(0, o_y)
    along_z(0, o_y)
    send(0, X, o_y)
    got(1, o_x)
    along_z(1, o_x)
    send(1, Y, o_x)

    loop(1, n, lambda d: x_wait(d).wait_recv())

    def xt_copy(d, t):
        return pltpu.make_async_remote_copy(
            src_ref=XN.at[t], dst_ref=XN.at[t],
            send_sem=xt_send.at[d], recv_sem=xt_recv.at[t],
            device_id={"tp": (mt + d) % tp}, device_id_type=pl.DeviceIdType.MESH,
        )

    for d in range(1, tp):
        xt_copy(d, mt).start()
    for d in range(1, tp):
        xt_copy(d, (mt + d) % tp).wait_recv()
    first = me * depth
    holder, offset = first // wl, first % wl
    for j in range(n):
        XM[pl.ds(j, 1), :] = XN[holder, j]
    pick = (
        lax.broadcasted_iota(jnp.int32, (wl, depth), 0)
        == offset + lax.broadcasted_iota(jnp.int32, (wl, depth), 1)
    )
    chosen = jnp.dot(
        XM[...].astype(BF16), jnp.where(pick, 1.0, 0.0).astype(BF16), preferred_element_type=F32
    ).astype(BF16)
    rest[2].wait()
    partial = jnp.dot(chosen, wq_v[...], preferred_element_type=F32)
    for j in range(n):
        QS[j] = partial[j:j + 1, :]
    QR[me] = QS[me]

    def zero(i):
        acc[i // (rows // 128), pl.ds(pl.multiple_of((i % (rows // 128)) * 128, 128), 128), :] = (
            jnp.zeros((128, half), F32))

    loop(0, 4 * (rows // 128), zero)

    got(2, o_x)
    send(2, Y, o_x)
    got(3, o_y)
    send(3, X, o_y)

    def q_copy(d):
        dst = (me + d) % n
        return pltpu.make_async_remote_copy(
            src_ref=QS.at[dst], dst_ref=QR.at[me],
            send_sem=q_send.at[d], recv_sem=q_recv.at[me],
            device_id={"sp": dst}, device_id_type=pl.DeviceIdType.MESH,
        )

    def q_wait(d):
        src = (me + d) % n
        return pltpu.make_async_remote_copy(
            src_ref=QS.at[src], dst_ref=QR.at[src],
            send_sem=q_send.at[d], recv_sem=q_recv.at[src],
            device_id={"sp": src}, device_id_type=pl.DeviceIdType.MESH,
        )

    loop(1, n, lambda d: q_copy(d).start())

    rest[1].wait()
    for d in range(1, tp):
        p_wait(d).wait_recv()

    zlist = ((0, 0, 0, X), (1, 0, 0, Y), (2, 0, 0, X), (3, 0, 0, Y), (0, 1, 0, X), (1, 0, 1, Y))

    def relay(s):
        for c, fy, fx, across in zlist:
            yo = yf if fy else y
            xo = xf if fx else x
            for zo, valid, more, d in ((z - s, z - s >= 0, up_ok, UP), (z + s, z + s < L, down_ok, DOWN)):
                @pl.when(valid)
                def _(c=c, zo=zo, more=more, d=d, yo=yo, xo=xo, across=across):
                    o = at(zo, yo, xo)
                    got(c, o)

                    @pl.when(more)
                    def _():
                        send(c, d, o)

                    send(c, across, o)
        for zo, valid in ((z - s, z - s >= 0), (z + s, z + s < L)):
            @pl.when(valid)
            def _(zo=zo):
                send(2, Y, at(zo, y, x))
                send(3, X, at(zo, y, x))
                got(2, at(zo, y, xf))
                send(2, Y, at(zo, y, xf))
                got(3, at(zo, yf, x))
                send(3, X, at(zo, yf, x))

    R = min(rows, 256)

    def dots(zo):
        for c, order in ((0, ((y, xf), (yf, xf))), (1, ((yf, x), (yf, xf))),
                         (2, ((yf, x), (yf, xf))), (3, ((y, xf), (yf, xf)))):
            for yo, xo in order:
                got(c, at(zo, yo, xo))

        def tile(i):
            c, r = i // (rows // R), pl.ds(pl.multiple_of((i % (rows // R)) * R, R), R)
            p = pl.ds(pl.multiple_of(zo * plane, plane), plane)
            acc[c, r, :] += jnp.dot(PR[r, p], W[c, p, :], preferred_element_type=F32)

        loop(0, 4 * (rows // R), tile)

    def finish(s):
        @pl.when(z - s >= 0)
        def _():
            dots(z - s)

        @pl.when((z + s < L) & (s > 0))
        def _():
            dots(z + s)

    def step(s):
        relay(s)
        finish(s - 1)

    loop(1, L, step)

    loop(1, n, lambda d: q_wait(d).wait_recv())
    total = QR[0]
    for j in range(1, n):
        total = total + QR[j]
    total = jnp.broadcast_to(total, (8, cols))
    query = jnp.concatenate(
        [rotated(total[:, i:i + LANES], qcos[...], qsin[...]) for i in range(0, cols, LANES)], axis=1)
    maps = 2 * heads
    pad = max(maps, 16)
    query = jnp.broadcast_to(query[:1], (pad, cols))
    keep = (
        lax.broadcasted_iota(jnp.int32, (pad, cols), 0)
        == lax.broadcasted_iota(jnp.int32, (pad, cols), 1) // MAP_DIM
    )
    query = jnp.where(keep, query, 0.0).astype(BF16)
    rest[3].wait()
    rest[4].wait()

    finish(L - 1)

    def rotate_rows(i):
        r = pl.ds(pl.multiple_of(i * R, R), R)
        cosine, sine = ct[r, :], st[r, :]
        for j in range(0, cols, LANES):
            tile = acc[j // half, r, pl.ds(j % half, LANES)]
            ko[r, pl.ds(j, LANES)] = rotated(tile, cosine, sine).astype(BF16)

    loop(0, rows // R, rotate_rows)

    def value_rows(i):
        r = pl.ds(pl.multiple_of(i * R, R), R)
        for h in range(2):
            vo[r, pl.ds(h * half, half)] = acc[2 + h, r, :].astype(BF16)

    loop(0, rows // R, value_rows)
    k_copy = pltpu.make_async_copy(ko, k_out.at[0], loc.at[0])
    v_copy = pltpu.make_async_copy(vo, v_out.at[0], loc.at[1])
    k_copy.start()
    v_copy.start()
    scores = lax.dot_general(
        query, ko[...], (((1,), (1,)), ((), ())), preferred_element_type=F32) * MAP_DIM ** -0.5
    weights = jnp.exp(scores - jnp.max(scores, axis=-1, keepdims=True))
    weights = weights / jnp.sum(weights, axis=-1, keepdims=True)
    high = weights.astype(BF16)
    left = weights - high.astype(F32)
    mid = left.astype(BF16)
    low = (left - mid.astype(F32)).astype(BF16)
    mixed = jnp.dot(jnp.concatenate([high, mid, low], axis=0), vo[...], preferred_element_type=F32)
    mixed = mixed[:pad] + mixed[pad:2 * pad] + mixed[2 * pad:]
    for h in range(heads):
        c = slice(h * VAL_DIM, (h + 1) * VAL_DIM)
        diff = mixed[2 * h:2 * h + 1, c] - lam[h] * mixed[2 * h + 1:2 * h + 2, c]
        normed = diff * lax.rsqrt(jnp.mean(diff * diff, axis=-1, keepdims=True) + norm_eps)
        read_out[0, pl.ds(h, 1), :] = normed * gain[...]
    k_copy.wait()
    v_copy.wait()

    loop(1, n, lambda d: x_copy(d).wait_send())
    loop(1, n, lambda d: q_copy(d).wait_send())
    for d in range(1, tp):
        p_copy(d).wait_send()
        xt_copy(d, mt).wait_send()
    copy(0, Y, me).wait_send()
    copy(1, X, me).wait_send()

    def sent(zo):
        a, ay, ax = at(zo, y, x), at(zo, yf, x), at(zo, y, xf)
        for c, o in ((0, a), (0, ay), (2, a), (3, a), (3, ay)):
            copy(c, X, o).wait_send()
        for c, o in ((1, a), (1, ax), (3, a), (2, a), (2, ax)):
            copy(c, Y, o).wait_send()
        for ok, d in ((up_ok & (zo <= z), UP), (down_ok & (zo >= z), DOWN)):
            @pl.when(ok)
            def _(d=d):
                for c, o in ((0, a), (0, ay), (1, a), (1, ax), (2, a), (3, a)):
                    copy(c, d, o).wait_send()

    loop(0, L, sent)


def body(n, tp, prompt, new_input, w_query, w_key, w_value, lam, out_gain):
    seqs, rows, wl = prompt.shape
    depth, cols = w_key.shape
    heads = lam.shape[0]
    half = cols // 2
    cos_t, sin_t = tables(jnp.arange(rows, dtype=F32))
    qcos, qsin = tables(jnp.full((1,), rows, F32))
    any_ = pl.BlockSpec(memory_space=pl.ANY)
    vmem = pl.BlockSpec(memory_space=pltpu.VMEM)
    smem = pl.BlockSpec(memory_space=pltpu.SMEM)
    dma = pltpu.SemaphoreType.DMA
    keys, values, read = pl.pallas_call(
        functools.partial(kernel, n, tp),
        out_shape=(
            jax.ShapeDtypeStruct((seqs, rows, cols), BF16),
            jax.ShapeDtypeStruct((seqs, rows, cols), BF16),
            jax.ShapeDtypeStruct((seqs, heads, VAL_DIM), F32),
        ),
        in_specs=[any_] * 7 + [vmem, vmem, smem, vmem],
        out_specs=(any_, any_, vmem),
        scratch_shapes=[
            pltpu.VMEM((4, n * depth, half), BF16),
            pltpu.VMEM((rows, tp * wl), BF16),
            pltpu.VMEM((4, rows, half), F32),
            pltpu.VMEM((rows, cols), BF16),
            pltpu.VMEM((rows, cols), BF16),
            pltpu.VMEM((tp, n, 1, wl), F32),
            pltpu.VMEM((n, wl), F32),
            pltpu.VMEM((depth, cols), BF16),
            pltpu.VMEM((n, 1, cols), F32),
            pltpu.VMEM((n, 1, cols), F32),
            pltpu.VMEM((rows, LANES), F32),
            pltpu.VMEM((rows, LANES), F32),
            dma((4 * n,)), dma((16 * n,)), dma((tp,)), dma((tp,)), dma((n,)), dma((n,)),
            dma((tp,)), dma((tp,)), dma((n,)), dma((n,)), dma((9,)),
        ],
        compiler_params=pltpu.CompilerParams(
            collective_id=0, has_side_effects=True, vmem_limit_bytes=56 * 1024 * 1024),
        name="prefill",
    )(
        prompt, new_input.astype(F32), w_query, w_key, w_value, cos_t, sin_t,
        jnp.broadcast_to(qcos, (8, LANES)), jnp.broadcast_to(qsin, (8, LANES)), lam, out_gain[None, :],
    )
    return keys, values, read.astype(BF16)


def solution(mesh):
    in_specs = (
        P("sp", None, "tp"), P("sp", "tp"), P("sp", "tp"), P("sp", "tp"), P("sp", "tp"), P("tp"), P(),
    )
    out_specs = (P("sp", None, "tp"), P("sp", None, "tp"), P("sp", "tp", None))
    return jax.shard_map(
        functools.partial(body, mesh.shape["sp"], mesh.shape["tp"]),
        mesh=mesh, in_specs=in_specs, out_specs=out_specs, check_vma=False)
```

time: 298 us -> 97.5 us (0.33)
  waiting for transfers between devices: 241 us -> 0 us
  Pallas kernels: 0 us -> 84.2 us
  matrix products: 21.7 us -> 0 us
  between operations: 13.9 us -> 0.66 us
  local copies, waits for them, and re-layouts: 16.1 us -> 5.75 us
  other arithmetic: 2.87 us -> 6.62 us
    all_gather x4 -> x0, waiting for transfers between devices: 239 us -> none  [the longest x1 84.1 us: body(): lax.all_gather(w_query, 'sp', axis=0, tiled=True)]
    pallas_call x0 -> x1, Pallas kernels: none -> 84.2 us  [body(): pl.pallas_call(functools.partial(kernel, n, tp), out_shape=(jax.ShapeDtyp...]
    dot_general x5 -> x0, matrix products: 21.7 us -> none  [the longest x1 8.02 us: body(): jnp.dot(row_piece, full_value, preferred_element_type=jnp.float32)]
    dot_general x1 -> x0, local copies, waits for them, and re-layouts: 6.5 us -> none  [body(): key_sum = jnp.dot(row_piece, full_key, preferred_element_type=jnp.float32)]
    unnamed x9 -> x4, local copies, waits for them, and re-layouts: 9.62 us -> 4.55 us
  transfers between devices with their start and end apart: 4 -> 0, of which waited for: 4 -> 0; matrix products, arithmetic and copies ran while one was open for 7% -> 0% of each run, Pallas kernels for 0% -> 0%
where the time goes in v1:
time: 97.5 us; the launch traced here: 97.2 us
  Pallas kernels  84.2 us (86%)
  other arithmetic  6.62 us (7%)
  local copies, waits for them, and re-layouts  5.75 us (6%)
    pallas_call x1, Pallas kernels, body(): pl.pallas_call(functools.partial(kernel, n, tp), out_shape=(jax.ShapeDtyp...  84.2 us
    unnamed x4, local copies, waits for them, and re-layouts  4.55 us
    neg x1, other arithmetic, tables(): -sine  1.96 us

profile of v1, /device:TPU:0, one launch (start us, length us, event | category | flops | bytes accessed | tf_op | source)
XLA Modules:
  0.0 97.2 jit_solution(16051089468734104241)
XLA Ops:
  0.6 0.1 fusion.4
  0.7 0.1 maximum_bitcast_fusion
  0.8 0.1 fusion.3
  0.8 0.1 maximum_bitcast_fusion.1
  0.9 0.6 broadcast_in_dim.23.qsin
  1.5 0.6 broadcast_in_dim.21.qcos
  2.1 1.3 %convert_element_type.6.fresh = f32[1,1024]{1,0:T(1,128)} convert(bf16[1,1024]{1,0:T(2,128)(2,1)} %param.8) | non-fusion elementwise | flops 1024 | bytes 6144 | tf_op jit(solution)/shard_map/convert_element_type | solution.py:422
  3.4 2.0 %fusion.2 = (f32[1024,32]{1,0:T(8,128)S(1)}, f32[1024,32]{1,0:T(8,128)S(1)}, f32[1024,32]{1,0:T(8,128)S(1)}) fusion(f32[32]{0:T(128)S(1)} %negate_power_fusion), kind=kLoop, calls=%fused_computation.5 | loop fusion | flops 65536 | bytes 393344 | tf_op jit(solution)/shard_map/neg | solution.py:30
  5.4 1.8 %pad_maximum_fusion = (f32[1024,128]{1,0:T(8,128)}, f32[1024,128]{1,0:T(8,128)}) fusion(f32[1024,32]{1,0:T(8,128)S(1)} %get-tuple-element.11, f32[1024,32]{1,0:T(8,128)S(1)} %get-tuple-element.10, f32[1024,32]{1,0:T(8,128)S(1)} %get-tuple-element.9), kind=kLoop, calls=%fused_computation | loop fusion | flops 786432 | bytes 1441792 | tf_op jit(solution)/shard_map/concatenate | solution.py:29
  7.2 84.2 %prefill.1 = (bf16[1,1024,1024]{2,1,0:T(8,128)(2,1)}, bf16[1,1024,1024]{2,1,0:T(8,128)(2,1)}, f32[1,8,128]{2,1,0:T(8,128)}) custom-call(bf16[1,1024,1024]{2,1,0:T(8,128)(2,1)} %prompt.1, f32[1,1024]{1,0:T(1,128)} %convert_element_type.6.fresh, bf16[128,1024]{1,0:T(8,128)(2,1)} %wq.1, bf16[128,1024]{1,0:T(8,128)(2,1)} %wk.1, bf16[128,1024]{1,0:T(8,128)(2,1)} %wv.1, ...), custom_call_target="tpu_custom_call" | custom-call | tf_op jit(solution)/shard_map/prefill/pallas_call | solution.py:393
  91.4 1.3 %convert_element_type.7 = bf16[1,8,128]{2,1,0:T(8,128)(2,1)} convert(f32[1,8,128]{2,1,0:T(8,128)} %get-tuple-element.8) | non-fusion elementwise | flops 1024 | bytes 6144 | tf_op jit(solution)/shard_map/convert_element_type | solution.py:425
  92.6 0.0 copy-start
  92.6 3.2 %copy.12 = bf16[1,1024,1024]{2,1,0:T(8,128)(2,1)} copy(bf16[1,1024,1024]{2,1,0:T(8,128)(2,1)} %get-tuple-element.19) | data formatting | bytes 4194304
  95.9 0.0 copy-done
  95.9 1.3 %copy.13 = bf16[1,1024,1024]{2,1,0:T(8,128)(2,1)} copy(bf16[1,1024,1024]{2,1,0:T(8,128)(2,1)S(1)} %copy-done) | data formatting | bytes 4194304
  (1 shorter events, 0.0 us)
Async XLA Ops:
  92.6 3.2 %copy-start = (bf16[1,1024,1024]{2,1,0:T(8,128)(2,1)S(1)}, bf16[1,1024,1024]{2,1,0:T(8,128)(2,1)}, u32[]{:S(2)}) copy-start(bf16[1,1024,1024]{2,1,0:T(8,128)(2,1)} %get-tuple-element.20) | copy-start | bytes 6291460

commit v2 on v1

--- a/solution.py
+++ b/solution.py
@@ -21,14 +21,11 @@
     return rope_base ** (-(jnp.arange(MAP_DIM // 2, dtype=F32) * 2.0 / MAP_DIM))
 
 
-def tables(positions):
-    angle = positions[:, None] * inverse_freq()
-    cosine, sine = jnp.cos(angle), jnp.sin(angle)
-    reps = LANES // MAP_DIM
-    return (
-        jnp.concatenate([cosine, cosine] * reps, axis=-1),
-        jnp.concatenate([-sine, sine] * reps, axis=-1),
-    )
+def table(position, inverse):
+    angle = position * inverse
+    lane = lax.broadcasted_iota(jnp.int32, angle.shape, 1) % MAP_DIM
+    sine = jnp.sin(angle)
+    return jnp.cos(angle), jnp.where(lane < MAP_DIM // 2, -sine, sine)
 
 
 def rotated(tile, cosine, sine):
@@ -39,10 +36,10 @@
 
 
 def kernel(
-    n, tp, prompt, fresh, wq, wk, wv, cos_t, sin_t, qcos, qsin, lam, gain,
-    k_out, v_out, read_out,
-    W, PR, acc, ko, vo, XN, XM, wq_v, QS, QR, ct, st,
-    w_recv, w_send, p_recv, p_send, x_recv, x_send, xt_recv, xt_send, q_recv, q_send, loc,
+    n, tp, prompt, fresh, wq, wk, wv, inverse,
+    k_out, v_out, q_out,
+    W, PR, acc, ko, vo, fr, XN, XM, wq_v, QS, QR, ct, st,
+    w_recv, w_send, p_recv, p_send, x_recv, x_send, xt_recv, xt_send, q_recv, q_send, loc, token,
 ):
     _, rows, wl = prompt.shape
     depth, cols = wk.shape
@@ -80,12 +77,16 @@
         pl.semaphore_signal(
             barrier, inc=1, device_id={"tp": (mt + d) % tp}, device_id_type=pl.DeviceIdType.MESH)
 
-    def greet(d, _):
+    up_ok, down_ok = z + 1 < L, z > 0
+
+    def signal(sem, d):
         pl.semaphore_signal(
-            barrier, inc=1, device_id={"sp": (me + d) % n}, device_id_type=pl.DeviceIdType.MESH)
-        return _
-
-    lax.fori_loop(1, n, greet, 0)
+            sem, inc=1, device_id={"sp": partner[d]}, device_id_type=pl.DeviceIdType.MESH)
+
+    signal(barrier, X)
+    signal(barrier, Y)
+    pl.when(up_ok)(lambda: signal(barrier, UP))
+    pl.when(down_ok)(lambda: signal(barrier, DOWN))
 
     def columns(t):
         return PR.at[:, pl.ds(pl.multiple_of(t * wl, wl), wl)]
@@ -95,11 +96,9 @@
         for i, w in enumerate((wk, wv)) for h in range(2)
     ]
     rest = [
-        pltpu.make_async_copy(fresh, XN.at[mt, me], loc.at[4]),
+        pltpu.make_async_copy(fresh, fr, loc.at[4]),
         pltpu.make_async_copy(prompt.at[0], columns(mt), loc.at[5]),
         pltpu.make_async_copy(wq, wq_v, loc.at[6]),
-        pltpu.make_async_copy(cos_t, ct, loc.at[7]),
-        pltpu.make_async_copy(sin_t, st, loc.at[8]),
     ]
     rest[0].start()
     for c in own:
@@ -107,9 +106,19 @@
     for c in rest[1:]:
         c.start()
     rest[0].wait()
+    XN[mt, me] = fr[...].astype(F32)
     for c in own:
         c.wait()
-    pl.semaphore_wait(barrier, n - 1 + tp - 1)
+
+    @pl.when(up_ok & down_ok)
+    def _():
+        pl.semaphore_wait(barrier, 4 + tp - 1)
+
+    @pl.when(jnp.logical_not(up_ok & down_ok))
+    def _():
+        pl.semaphore_wait(barrier, 3 + tp - 1)
+
+    signal(token.at[Y], Y)
 
     def x_copy(d):
         return pltpu.make_async_remote_copy(
@@ -128,10 +137,6 @@
 
     def loop(lo, hi, f):
         lax.fori_loop(lo, hi, lambda i, _: (f(i), _)[1], 0)
-
-    loop(1, n, lambda d: x_copy(d).start())
-
-    up_ok, down_ok = z + 1 < L, z > 0
 
     def along_z(c, o):
         @pl.when(up_ok)
@@ -144,7 +149,7 @@
 
     send(0, Y, me)
     send(1, X, me)
-    for c in range(4):
+    for c in (2, 3, 0, 1):
         along_z(c, me)
     send(2, X, me)
     send(3, Y, me)
@@ -170,6 +175,19 @@
 
     for d in range(1, tp):
         p_copy(d).start()
+
+    pl.semaphore_wait(token.at[Y], 1)
+    signal(token.at[X], X)
+    pl.semaphore_wait(token.at[X], 1)
+    for ok, more, d in ((down_ok, up_ok, UP), (up_ok, down_ok, DOWN)):
+        @pl.when(ok)
+        def _(d=d):
+            pl.semaphore_wait(token.at[d], 1)
+
+        @pl.when(more)
+        def _(d=d):
+            signal(token.at[d], d)
+    loop(1, n, lambda d: x_copy(d).start())
 
     o_y, o_x = at(z, yf, x), at(z, y, xf)
     got(0, o_y)
@@ -215,6 +233,14 @@
 
     loop(0, 4 * (rows // 128), zero)
 
+    def angles(i):
+        position = (i * 64 + lax.broadcasted_iota(jnp.int32, (64, LANES), 0)).astype(F32)
+        r = pl.ds(pl.multiple_of(i * 64, 64), 64)
+        ct[r, :], st[r, :] = table(position, inverse[...])
+
+    loop(0, rows // 64, angles)
+    qcos, qsin = table(jnp.full((8, LANES), rows, F32), inverse[...])
+
     got(2, o_x)
     send(2, Y, o_x)
     got(3, o_y)
@@ -242,15 +268,13 @@
     for d in range(1, tp):
         p_wait(d).wait_recv()
 
-    zlist = ((0, 0, 0, X), (1, 0, 0, Y), (2, 0, 0, X), (3, 0, 0, Y), (0, 1, 0, X), (1, 0, 1, Y))
-
     def relay(s):
-        for c, fy, fx, across in zlist:
-            yo = yf if fy else y
-            xo = xf if fx else x
-            for zo, valid, more, d in ((z - s, z - s >= 0, up_ok, UP), (z + s, z + s < L, down_ok, DOWN)):
+        sides = ((z - s, z - s >= 0, up_ok, UP), (z + s, z + s < L, down_ok, DOWN))
+
+        def along(c, yo, xo, across):
+            for zo, valid, more, d in sides:
                 @pl.when(valid)
-                def _(c=c, zo=zo, more=more, d=d, yo=yo, xo=xo, across=across):
+                def _(zo=zo, more=more, d=d):
                     o = at(zo, yo, xo)
                     got(c, o)
 
@@ -258,31 +282,37 @@
                     def _():
                         send(c, d, o)
 
-                    send(c, across, o)
-        for zo, valid in ((z - s, z - s >= 0), (z + s, z + s < L)):
+                    for a in across:
+                        send(c, a, o)
+
+        along(2, y, x, (X, Y))
+        along(3, y, x, (Y, X))
+        along(0, y, x, (X,))
+        along(1, y, x, (Y,))
+        for zo, valid, _, _ in sides:
             @pl.when(valid)
             def _(zo=zo):
-                send(2, Y, at(zo, y, x))
-                send(3, X, at(zo, y, x))
                 got(2, at(zo, y, xf))
                 send(2, Y, at(zo, y, xf))
                 got(3, at(zo, yf, x))
                 send(3, X, at(zo, yf, x))
+        along(0, yf, x, (X,))
+        along(1, y, xf, (Y,))
 
     R = min(rows, 256)
 
     def dots(zo):
-        for c, order in ((0, ((y, xf), (yf, xf))), (1, ((yf, x), (yf, xf))),
-                         (2, ((yf, x), (yf, xf))), (3, ((y, xf), (yf, xf)))):
+        for c, order in ((2, ((yf, x), (yf, xf))), (3, ((y, xf), (yf, xf))),
+                         (0, ((y, xf), (yf, xf))), (1, ((yf, x), (yf, xf)))):
             for yo, xo in order:
                 got(c, at(zo, yo, xo))
 
-        def tile(i):
-            c, r = i // (rows // R), pl.ds(pl.multiple_of((i % (rows // R)) * R, R), R)
-            p = pl.ds(pl.multiple_of(zo * plane, plane), plane)
-            acc[c, r, :] += jnp.dot(PR[r, p], W[c, p, :], preferred_element_type=F32)
-
-        loop(0, 4 * (rows // R), tile)
+            def tile(i, c=c):
+                r = pl.ds(pl.multiple_of(i * R, R), R)
+                p = pl.ds(pl.multiple_of(zo * plane, plane), plane)
+                acc[c, r, :] += jnp.dot(PR[r, p], W[c, p, :], preferred_element_type=F32)
+
+            loop(0, rows // R, tile)
 
     def finish(s):
         @pl.when(z - s >= 0)
@@ -305,7 +335,7 @@
         total = total + QR[j]
     total = jnp.broadcast_to(total, (8, cols))
     query = jnp.concatenate(
-        [rotated(total[:, i:i + LANES], qcos[...], qsin[...]) for i in range(0, cols, LANES)], axis=1)
+        [rotated(total[:, i:i + LANES], qcos, qsin) for i in range(0, cols, LANES)], axis=1)
     maps = 2 * heads
     pad = max(maps, 16)
     query = jnp.broadcast_to(query[:1], (pad, cols))
@@ -313,9 +343,7 @@
         lax.broadcasted_iota(jnp.int32, (pad, cols), 0)
         == lax.broadcasted_iota(jnp.int32, (pad, cols), 1) // MAP_DIM
     )
-    query = jnp.where(keep, query, 0.0).astype(BF16)
-    rest[3].wait()
-    rest[4].wait()
+    q_out[...] = jnp.where(keep, query, 0.0).astype(BF16)
 
     finish(L - 1)
 
@@ -326,35 +354,17 @@
             tile = acc[j // half, r, pl.ds(j % half, LANES)]
             ko[r, pl.ds(j, LANES)] = rotated(tile, cosine, sine).astype(BF16)
 
-    loop(0, rows // R, rotate_rows)
-
     def value_rows(i):
         r = pl.ds(pl.multiple_of(i * R, R), R)
         for h in range(2):
             vo[r, pl.ds(h * half, half)] = acc[2 + h, r, :].astype(BF16)
 
+    v_copy = pltpu.make_async_copy(vo, v_out.at[0], loc.at[1])
+    k_copy = pltpu.make_async_copy(ko, k_out.at[0], loc.at[0])
     loop(0, rows // R, value_rows)
-    k_copy = pltpu.make_async_copy(ko, k_out.at[0], loc.at[0])
-    v_copy = pltpu.make_async_copy(vo, v_out.at[0], loc.at[1])
+    v_copy.start()
+    loop(0, rows // R, rotate_rows)
     k_copy.start()
-    v_copy.start()
-    scores = lax.dot_general(
-        query, ko[...], (((1,), (1,)), ((), ())), preferred_element_type=F32) * MAP_DIM ** -0.5
-    weights = jnp.exp(scores - jnp.max(scores, axis=-1, keepdims=True))
-    weights = weights / jnp.sum(weights, axis=-1, keepdims=True)
-    high = weights.astype(BF16)
-    left = weights - high.astype(F32)
-    mid = left.astype(BF16)
-    low = (left - mid.astype(F32)).astype(BF16)
-    mixed = jnp.dot(jnp.concatenate([high, mid, low], axis=0), vo[...], preferred_element_type=F32)
-    mixed = mixed[:pad] + mixed[pad:2 * pad] + mixed[2 * pad:]
-    for h in range(heads):
-        c = slice(h * VAL_DIM, (h + 1) * VAL_DIM)
-        diff = mixed[2 * h:2 * h + 1, c] - lam[h] * mixed[2 * h + 1:2 * h + 2, c]
-        normed = diff * lax.rsqrt(jnp.mean(diff * diff, axis=-1, keepdims=True) + norm_eps)
-        read_out[0, pl.ds(h, 1), :] = normed * gain[...]
-    k_copy.wait()
-    v_copy.wait()
 
     loop(1, n, lambda d: x_copy(d).wait_send())
     loop(1, n, lambda d: q_copy(d).wait_send())
@@ -377,6 +387,41 @@
                     copy(c, d, o).wait_send()
 
     loop(0, L, sent)
+    v_copy.wait()
+    k_copy.wait()
+
+
+def read(keys, values, query, lam, gain, k_out, v_out, read_out, ko, vo, sem):
+    heads, pad = lam.shape[0], query.shape[0]
+    v_in = pltpu.make_async_copy(values.at[0], vo, sem.at[1])
+    k_in = pltpu.make_async_copy(keys.at[0], ko, sem.at[0])
+    k_copy = pltpu.make_async_copy(ko, k_out.at[0], sem.at[2])
+    v_copy = pltpu.make_async_copy(vo, v_out.at[0], sem.at[3])
+    k_in.start()
+    v_in.start()
+    k_in.wait()
+    k_copy.start()
+    scores = lax.dot_general(
+        query[...], ko[...], (((1,), (1,)), ((), ())), preferred_element_type=F32) * MAP_DIM ** -0.5
+    weights = jnp.exp(scores - jnp.max(scores, axis=-1, keepdims=True))
+    weights = weights / jnp.sum(weights, axis=-1, keepdims=True)
+    high = weights.astype(BF16)
+    left = weights - high.astype(F32)
+    mid = left.astype(BF16)
+    low = (left - mid.astype(F32)).astype(BF16)
+    v_in.wait()
+    v_copy.start()
+    mixed = jnp.dot(jnp.concatenate([high, mid, low], axis=0), vo[...], preferred_element_type=F32)
+    mixed = mixed[:pad] + mixed[pad:2 * pad] + mixed[2 * pad:]
+    reads = []
+    for h in range(heads):
+        c = slice(h * VAL_DIM, (h + 1) * VAL_DIM)
+        diff = mixed[2 * h:2 * h + 1, c] - lam[h] * mixed[2 * h + 1:2 * h + 2, c]
+        normed = diff * lax.rsqrt(jnp.mean(diff * diff, axis=-1, keepdims=True) + norm_eps)
+        reads.append(normed * gain[...])
+    read_out[0] = jnp.concatenate(reads, axis=0).astype(BF16)
+    k_copy.wait()
+    v_copy.wait()
 
 
 def body(n, tp, prompt, new_input, w_query, w_key, w_value, lam, out_gain):
@@ -384,20 +429,21 @@
     depth, cols = w_key.shape
     heads = lam.shape[0]
     half = cols // 2
-    cos_t, sin_t = tables(jnp.arange(rows, dtype=F32))
-    qcos, qsin = tables(jnp.full((1,), rows, F32))
+    pad = max(2 * heads, 16)
+    inverse = jnp.tile(inverse_freq(), LANES * 2 // MAP_DIM)[None, :]
     any_ = pl.BlockSpec(memory_space=pl.ANY)
+    hbm = pl.BlockSpec(memory_space=pltpu.HBM)
     vmem = pl.BlockSpec(memory_space=pltpu.VMEM)
     smem = pl.BlockSpec(memory_space=pltpu.SMEM)
     dma = pltpu.SemaphoreType.DMA
-    keys, values, read = pl.pallas_call(
+    keys, values, query = pl.pallas_call(
         functools.partial(kernel, n, tp),
         out_shape=(
             jax.ShapeDtypeStruct((seqs, rows, cols), BF16),
             jax.ShapeDtypeStruct((seqs, rows, cols), BF16),
-            jax.ShapeDtypeStruct((seqs, heads, VAL_DIM), F32),
+            jax.ShapeDtypeStruct((pad, cols), BF16),
         ),
-        in_specs=[any_] * 7 + [vmem, vmem, smem, vmem],
+        in_specs=[hbm] * 5 + [vmem],
         out_specs=(any_, any_, vmem),
         scratch_shapes=[
             pltpu.VMEM((4, n * depth, half), BF16),
@@ -405,6 +451,7 @@
             pltpu.VMEM((4, rows, half), F32),
             pltpu.VMEM((rows, cols), BF16),
             pltpu.VMEM((rows, cols), BF16),
+            pltpu.VMEM((1, wl), BF16),
             pltpu.VMEM((tp, n, 1, wl), F32),
             pltpu.VMEM((n, wl), F32),
             pltpu.VMEM((depth, cols), BF16),
@@ -413,16 +460,25 @@
             pltpu.VMEM((rows, LANES), F32),
             pltpu.VMEM((rows, LANES), F32),
             dma((4 * n,)), dma((16 * n,)), dma((tp,)), dma((tp,)), dma((n,)), dma((n,)),
-            dma((tp,)), dma((tp,)), dma((n,)), dma((n,)), dma((9,)),
+            dma((tp,)), dma((tp,)), dma((n,)), dma((n,)), dma((7,)), pltpu.SemaphoreType.REGULAR((4,)),
         ],
         compiler_params=pltpu.CompilerParams(
-            collective_id=0, has_side_effects=True, vmem_limit_bytes=56 * 1024 * 1024),
+            collective_id=0, has_side_effects=True, vmem_limit_bytes=40 * 1024 * 1024),
         name="prefill",
-    )(
-        prompt, new_input.astype(F32), w_query, w_key, w_value, cos_t, sin_t,
-        jnp.broadcast_to(qcos, (8, LANES)), jnp.broadcast_to(qsin, (8, LANES)), lam, out_gain[None, :],
-    )
-    return keys, values, read.astype(BF16)
+    )(prompt, new_input, w_query, w_key, w_value, inverse)
+    return pl.pallas_call(
+        read,
+        out_shape=(
+            jax.ShapeDtypeStruct((seqs, rows, cols), BF16),
+            jax.ShapeDtypeStruct((seqs, rows, cols), BF16),
+            jax.ShapeDtypeStruct((seqs, heads, VAL_DIM), BF16),
+        ),
+        in_specs=[any_, any_, vmem, smem, vmem],
+        out_specs=(any_, any_, vmem),
+        scratch_shapes=[pltpu.VMEM((rows, cols), BF16), pltpu.VMEM((rows, cols), BF16), dma((4,))],
+        compiler_params=pltpu.CompilerParams(vmem_limit_bytes=24 * 1024 * 1024),
+        name="read",
+    )(keys, values, query, lam, out_gain[None, :])
 
 
 def solution(mesh):

time: 97.5 us -> 98.3 us (level)
  Pallas kernels: 84.2 us -> 92 us
  other arithmetic: 6.62 us -> 0.01 us
    pallas_call x1, Pallas kernels: 84.2 us -> 88.3 us  [body(): pl.pallas_call(functools.partial(kernel, n, tp), out_shape=(jax.ShapeDtyp...]
    pallas_call x0 -> x1, Pallas kernels: none -> 3.62 us  [body(): pl.pallas_call(read, out_shape=(jax.ShapeDtypeStruct((seqs, rows, cols),...]
    convert_element_type x2 -> x0, other arithmetic: 2.54 us -> none  [the longest x1 1.28 us: body(): new_input.astype(F32)]
    neg x1 -> x0, other arithmetic: 1.96 us -> none  [tables(): -sine]
    concatenate x1 -> x0, other arithmetic: 1.85 us -> none  [tables(): jnp.concatenate([cosine, cosine] * reps, axis=-1)]
    broadcast_in_dim x2 -> x0, local copies, waits for them, and re-layouts: 1.2 us -> none  [the longest x1 0.61 us: body(): jnp.broadcast_to(qsin, (8, LANES))]
    unnamed x4 -> x14, local copies, waits for them, and re-layouts: 4.55 us -> 5.14 us
where the time goes in v2:
time: 98.3 us; the launch traced here: 97.9 us
  Pallas kernels  92 us (94%)
  local copies, waits for them, and re-layouts  5.22 us (5%)
    pallas_call x1, Pallas kernels, body(): pl.pallas_call(functools.partial(kernel, n, tp), out_shape=(jax.ShapeDtyp...  88.3 us
    unnamed x14, local copies, waits for them, and re-layouts  5.14 us
    pallas_call x1, Pallas kernels, body(): pl.pallas_call(read, out_shape=(jax.ShapeDtypeStruct((seqs, rows, cols),...  3.62 us

profile of v2, /device:TPU:0, one launch (start us, length us, event | category | flops | bytes accessed | tf_op | source)
XLA Modules:
  0.0 97.9 jit_solution(13074862297864460107)
XLA Ops:
  0.6 0.0 copy-start.6
  0.6 0.0 copy-start.5
  0.7 0.1 broadcast_in_dim_tile.3.inverse
  0.8 0.0 copy-start
  0.8 1.6 %copy-done = bf16[1,1024,1024]{2,1,0:T(8,128)(2,1)S(1)} copy-done((bf16[1,1024,1024]{2,1,0:T(8,128)(2,1)S(1)}, bf16[1,1024,1024]{2,1,0:T(8,128)(2,1)}, u32[]{:S(2)}) %copy-start) | copy-done | bytes 2097176
  2.4 0.0 copy-start.1
  2.4 0.9 copy-done.1
  3.3 0.0 copy-start.2
  3.3 0.9 copy-done.2
  4.3 0.0 copy-start.3
  4.3 0.9 copy-done.3
  5.2 0.0 copy-start.4
  5.2 0.7 copy-done.4
  5.9 88.3 %prefill.1 = (bf16[1,1024,1024]{2,1,0:T(8,128)(2,1)S(1)}, bf16[1,1024,1024]{2,1,0:T(8,128)(2,1)S(1)}, bf16[16,1024]{1,0:T(8,128)(2,1)S(1)}) custom-call(bf16[1,1024,1024]{2,1,0:T(8,128)(2,1)S(1)} %copy-done, bf16[1,1024]{1,0:T(2,128)(2,1)S(1)} %copy-done.4, bf16[128,1024]{1,0:T(8,128)(2,1)S(1)} %copy-done.1, bf16[128,1024]{1,0:T(8,128)(2,1)S(1)} %copy-done.2, ...), custom_call_target="tpu_custom_call" | custom-call | tf_op jit(solution)/shard_map/prefill/pallas_call | solution.py:439
  94.2 0.0 copy-done.6
  94.3 0.0 copy-done.5
  94.3 3.6 %read.1 = (bf16[1,1024,1024]{2,1,0:T(8,128)(2,1)}, bf16[1,1024,1024]{2,1,0:T(8,128)(2,1)}, bf16[1,8,128]{2,1,0:T(8,128)(2,1)}) custom-call(bf16[1,1024,1024]{2,1,0:T(8,128)(2,1)S(1)} %get-tuple-element.6.keys, bf16[1,1024,1024]{2,1,0:T(8,128)(2,1)S(1)} %get-tuple-element.7.values, bf16[16,1024]{1,0:T(8,128)(2,1)S(1)} %get-tuple-element.8.query, ...), custom_call_target="tpu_custom_call" | custom-call | tf_op jit(solution)/shard_map/read/pallas_call | solution.py:469
  (2 shorter events, 0.0 us)
Async XLA Ops:
  0.6 93.6 %copy-start.6 = (f32[128]{0:T(128)S(1)}, f32[128]{0:T(128)}, u32[]{:S(2)}) copy-start(f32[128]{0:T(128)} %param.13) | copy-start | bytes 1540
  0.6 93.6 %copy-start.5 = (f32[8]{0:T(128)S(1)}, f32[8]{0:T(128)}, u32[]{:S(2)}) copy-start(f32[8]{0:T(128)} %lam.1) | copy-start | bytes 100
  0.8 1.6 %copy-start = (bf16[1,1024,1024]{2,1,0:T(8,128)(2,1)S(1)}, bf16[1,1024,1024]{2,1,0:T(8,128)(2,1)}, u32[]{:S(2)}) copy-start(bf16[1,1024,1024]{2,1,0:T(8,128)(2,1)} %prompt.1) | copy-start | bytes 6291460
  2.4 0.9 copy-start.1
  3.3 0.9 copy-start.2
  4.3 0.9 copy-start.3
  5.2 0.7 copy-start.4
